TPU v7x, 32 devices: a whole 2x2x4 slice. The times are simulated.
32 devices in a mesh: grp: 2 (over y), fs: 4 (over z), tp: 4 (over x, core).
Axes of the slice: x: 2, y: 2, z: 4, core: 2. Of those that a mesh axis runs over, the one named last changes fastest.
Arguments:
- tokens: bfloat16 [6144, 2048], P(('grp', 'fs')), parts along dimension 0, may hold values from -6 to 6
- pre_gain: float32 [2048], replicated, may hold values from 0.1 to 1.9
- up_weight: bfloat16 [2048, 8192], P('fs', 'tp'), may hold values from -0.125 to 0.125
- down_weight: bfloat16 [8192, 2048], P(('tp', 'fs')), as said below
- post_gain: float32 [2048], P('tp'), may hold values from 0.1 to 1.9
Outputs:
- mixed: bfloat16 [6144, 2048], P(('grp', 'fs'), 'tp'), parts along dimension 0
There are 2 independent parts, one for each index of `grp`. A program takes and returns all parts, laid end to end along the dimension named above; an argument that names none is the same for every part. Nothing has to cross between parts.
Inputs may be any that keep to these rules, and one draw needn't show every extreme that they name: `down_weight`: a matrix whose columns fall into 4 consecutive blocks of different magnitudes.
All inputs are finite; a program needn't handle non-finite values.
Results may differ from a plain program's by a relative error of at most 0.014.
Values may be sent and summed in bfloat16 or wider, within the bound.
A program may use at most 64 MiB of HBM per device.

v0:
```python
import jax
import jax.numpy as jnp
from jax import lax
from jax.sharding import PartitionSpec as P


def shards(tokens, pre_gain, up_weight, down_weight, post_gain):
    eps = 1e-06
    values = tokens.astype(jnp.float32)
    normed = (
        values * lax.rsqrt(jnp.mean(values * values, axis=1, keepdims=True) + eps) * pre_gain
    ).astype(jnp.bfloat16)
    full_up = lax.all_gather(up_weight, "fs", axis=0, tiled=True)
    up = jnp.dot(normed, full_up, preferred_element_type=jnp.float32)
    hidden = jnp.square(jnp.maximum(up, 0.0)).astype(jnp.bfloat16)
    full_down = lax.all_gather(down_weight, "fs", axis=0, tiled=True)
    partial_terms = jnp.dot(hidden, full_down, preferred_element_type=jnp.float32)
    own_width = post_gain.shape[0]
    full_width = lax.axis_size("tp") * own_width
    mixed = lax.psum_scatter(
        partial_terms.astype(jnp.bfloat16), "tp", scatter_dimension=1, tiled=True
    ).astype(jnp.float32)
    squares = lax.psum(jnp.sum(mixed * mixed, axis=1), "tp")
    factor = lax.rsqrt(squares / full_width + eps)
    return (mixed * factor[:, None] * post_gain).astype(jnp.bfloat16)


def solution(mesh):
    in_specs = (P(("grp", "fs"), None), P(), P("fs", "tp"), P(("tp", "fs"), None), P("tp"))
    out_specs = P(("grp", "fs"), "tp")
    return jax.shard_map(shards, mesh=mesh, in_specs=in_specs, out_specs=out_specs, check_vma=False)
```

profile of v0, /device:TPU:0, one launch (start us, length us, event | category | flops | bytes accessed | tf_op | source)
XLA Modules:
  0.0 383.3 jit_solution(18431239371068029638)
XLA Ops:
  6.5 0.0 copy-start
  6.5 0.0 copy-start.2
  6.5 0.0 all-gather.3.cloned.1.call-start
  6.5 0.7 all-gather.3.cloned.1.call-update
  7.3 0.0 all-gather.5.cloned.1.call-start
  7.3 0.7 all-gather.5.cloned.1.call-update
  8.0 0.0 reduce-scatter.2.cloned.1.call-start
  8.1 0.4 copy-done
  8.4 0.7 fusion
  9.1 0.0 copy-start.1
  9.1 152.1 %all-gather.3.cloned.1.call-done = bf16[2048,2048]{1,0:T(8,128)(2,1)} async-done(((bf16[512,2048]{1,0:T(8,128)(2,1)}), bf16[2048,2048]{1,0:T(8,128)(2,1)}) %all-gather.3.cloned.1.call-update) | async-done | bytes 8388624 | tf_op jit(solution)/shard_map/all_gather | solution.py:13
  161.3 149.4 %all-gather.5.cloned.1.call-done = bf16[2048,2048]{1,0:T(8,128)(2,1)} async-done(((bf16[512,2048]{1,0:T(8,128)(2,1)}), bf16[2048,2048]{1,0:T(8,128)(2,1)}) %all-gather.5.cloned.1.call-update) | async-done | bytes 8388624 | tf_op jit(solution)/shard_map/all_gather | solution.py:16
  310.7 0.0 copy-done.2
  310.7 20.6 %convolution_convert_fusion = bf16[768,2048]{1,0:T(8,128)(2,1)} fusion(bf16[2048,2048]{1,0:T(8,128)(2,1)} %all-gather.5.cloned.1.call-done, bf16[2048,2048]{1,0:T(8,128)(2,1)} %all-gather.3.cloned.1.call-done, bf16[768,2048]{1,0:T(8,128)(2,1)S(1)} %copy-done, f32[2048]{0:T(1024)S(1)} %copy-done.2, f32[768]{0:T(1024)S(1)} %add_rsqrt_fusion.1), kind=kOutput, calls=%fused_computation.6 | convolution fusion | flops 12897484800 | bytes 23079936 | tf_op jit(solution)/shard_map/dot_general | solution.py:17
  331.3 0.0 reduce-scatter.2.cloned.1.call-update
  331.3 36.1 %reduce-scatter.2.cloned.1.call-done = bf16[768,512]{1,0:T(8,128)(2,1)} async-done(((bf16[768,2048]{1,0:T(8,128)(2,1)}), bf16[768,512]{1,0:T(8,128)(2,1)}) %reduce-scatter.2.cloned.1.call-update) | async-done | bytes 786448 | tf_op jit(solution)/shard_map/reduce_scatter | solution.py:20
  367.4 1.4 fusion.6
  368.7 5.8 %psum.7 = f32[768]{0:T(1024)S(1)} all-reduce(f32[768]{0:T(1024)S(1)} %fusion.6), channel_id=1, replica_groups=mesh['grp'=2,'fs'=4,'tp'=4] {'tp'}, use_global_device_ids=true, to_apply=%region_3.0 | all-reduce | flops 768 | bytes 6144 | tf_op jit(solution)/shard_map/psum | solution.py:23
  374.5 0.0 copy-done.1
  374.5 2.3 fusion.8
  (2 shorter events, 0.0 us)
Async XLA Ops:
  6.5 1.9 copy-start
  6.5 304.1 %copy-start.2 = (f32[2048]{0:T(1024)S(1)}, f32[2048]{0:T(1024)}, u32[]{:S(2)}) copy-start(f32[2048]{0:T(1024)} %param.6) | copy-start | bytes 24580
  6.5 154.7 %all-gather.3.cloned.1.call-start = ((), (), s32[]{:S(2)}) async-start(), calls=%async_computation.1 | async-start | bytes 10485760 | tf_op jit(solution)/shard_map/all_gather | solution.py:13
  7.3 303.4 %all-gather.5.cloned.1.call-start = ((), (), s32[]{:S(2)}) async-start(), calls=%async_computation.2 | async-start | bytes 10485760 | tf_op jit(solution)/shard_map/all_gather | solution.py:16
  8.0 359.3 %reduce-scatter.2.cloned.1.call-start = ((), (), s32[]{:S(2)}) async-start(), calls=%async_computation.3 | async-start | bytes 3932160 | tf_op jit(solution)/shard_map/reduce_scatter | solution.py:20
  9.1 365.4 %copy-start.1 = (f32[512]{0:T(512)S(1)}, f32[512]{0:T(512)}, u32[]{:S(2)}) copy-start(f32[512]{0:T(512)} %param.9) | copy-start | bytes 6148
Sparse Core Ops, SparseCore 0:
  8.9 152.3 all-gather.2
  162.8 147.7 all-gather.4
  331.4 35.8 reduce-scatter.1
where the time goes:
time: 383 us
  waiting for transfers between devices  339 us (89%)
  matrix products  20.6 us (5%)
  between operations  13.1 us (3%)
  blocking collectives  5.77 us (2%)
  other arithmetic  4.31 us (1%)
    all_gather x1, waiting for transfers between devices, shards(): full_up = lax.all_gather(up_weight, 'fs', axis=0, tiled=True)  152 us
    all_gather x1, waiting for transfers between devices, shards(): full_down = lax.all_gather(down_weight, 'fs', axis=0, tiled=True)  149 us
    reduce_scatter x1, waiting for transfers between devices, shards(): lax.psum_scatter(partial_terms.astype(jnp.bfloat16), 'tp', scatter_dimens...  36.1 us
    dot_general x1, matrix products, shards(): jnp.dot(hidden, full_down, preferred_element_type=jnp.float32)  20.6 us
  transfers between devices with their start and end apart: 3, of which 3 were waited for; matrix products, arithmetic and copies ran while one was open for 0% of the time, Pallas kernels for 0%

commit v1 on v0

v1 whole, which is shorter than its diff:
```python
import functools

import jax
import jax.numpy as jnp
from jax import lax
from jax.experimental import pallas as pl
from jax.experimental.pallas import tpu as pltpu
from jax.sharding import PartitionSpec as P

MESH = pl.DeviceIdType.MESH
EPS = 1e-06
LANES = 128


def layer_kernel(sizes, tok_hbm, gain_ref, up_hbm, down_hbm, out_ref,
                 tok, normed, ubuf, dbuf, hidden, sbuf, rbuf,
                 tok_sem, lup_sem, ldn_sem, zrecv, yrecv, zsend, ysend, rsend, rrecv):
    n_grp, n_fs, n_tp, p_up, p_dn, c_up = sizes
    per_grp = n_tp // n_grp
    pieces = p_up + p_dn
    grp = lax.axis_index("grp")
    me = lax.axis_index("fs")
    tp = lax.axis_index("tp")
    rows_up = up_hbm.shape[0]
    rows_dn = down_hbm.shape[0]
    own_width = p_dn * LANES

    def block(q, g, src):
        if q < p_up:
            return ubuf.at[q, g, pl.ds(pl.multiple_of(src * rows_up, rows_up), rows_up), :]
        return dbuf.at[q - p_up, g, pl.ds(pl.multiple_of(src * rows_dn, rows_dn), rows_dn), :]

    def local_copies(q, j):
        g = lax.rem(grp + j, n_grp)
        if q < p_up:
            cols = pl.ds(pl.multiple_of((q * n_grp + g) * c_up, LANES), c_up)
            return [pltpu.make_async_copy(up_hbm.at[:, cols], block(q, g, me), lup_sem.at[q, j])]
        copies = []
        for i in range(per_grp):
            start = (g * per_grp + i) * own_width + (q - p_up) * LANES
            cols = pl.ds(pl.multiple_of(start, LANES), LANES)
            dst = dbuf.at[q - p_up, g, pl.ds(pl.multiple_of(me * rows_dn, rows_dn), rows_dn),
                          pl.ds(i * LANES, LANES)]
            copies.append(pltpu.make_async_copy(
                down_hbm.at[:, cols], dst, ldn_sem.at[q - p_up, j, i]))
        return copies

    def z_copy(q, src, side):
        to = me + 1 if side else me - 1
        return pltpu.make_async_remote_copy(
            src_ref=block(q, grp, src), dst_ref=block(q, grp, src),
            send_sem=zsend.at[q, src], recv_sem=zrecv.at[q, src],
            device_id={"fs": to}, device_id_type=MESH)

    def z_own(q, side):
        to = me + 1 if side else me - 1
        return pltpu.make_async_remote_copy(
            src_ref=block(q, grp, me), dst_ref=block(q, grp, me),
            send_sem=zsend.at[q, me] if side else zsend.at[q, n_fs], recv_sem=zrecv.at[q, me],
            device_id={"fs": to}, device_id_type=MESH)

    def y_copy(q, src, j):
        to = lax.rem(grp + j, n_grp)
        return pltpu.make_async_remote_copy(
            src_ref=block(q, grp, src), dst_ref=block(q, grp, src),
            send_sem=ysend.at[q, j, src], recv_sem=yrecv.at[q, j, src],
            device_id={"grp": to}, device_id_type=MESH)

    def y_arrival(q, src, j):
        g = lax.rem(grp + n_grp - j, n_grp)
        return pltpu.make_async_remote_copy(
            src_ref=block(q, g, src), dst_ref=block(q, g, src),
            send_sem=ysend.at[q, j, src], recv_sem=yrecv.at[q, j, src],
            device_id={"grp": g}, device_id_type=MESH)

    def part_copy(q, j):
        to = lax.rem(tp + j, n_tp)
        return pltpu.make_async_remote_copy(
            src_ref=sbuf.at[q, to], dst_ref=rbuf.at[q, j - 1],
            send_sem=rsend.at[q, j - 1], recv_sem=rrecv.at[q, j - 1],
            device_id={"tp": to}, device_id_type=MESH)

    tok_copy = pltpu.make_async_copy(tok_hbm, tok, tok_sem)
    for q in range(pieces):
        for j in range(n_grp):
            for copy in local_copies(q, j):
                copy.start()
        if q == 0:
            tok_copy.start()

    barrier = pltpu.get_barrier_semaphore()

    @pl.when(me > 0)
    def _():
        pl.semaphore_signal(barrier, inc=1, device_id={"fs": me - 1}, device_id_type=MESH)

    @pl.when(me < n_fs - 1)
    def _():
        pl.semaphore_signal(barrier, inc=1, device_id={"fs": me + 1}, device_id_type=MESH)

    for j in range(1, n_grp):
        pl.semaphore_signal(barrier, inc=1, device_id={"grp": lax.rem(grp + j, n_grp)},
                            device_id_type=MESH)
    for j in range(1, n_tp):
        pl.semaphore_signal(barrier, inc=1, device_id={"tp": lax.rem(tp + j, n_tp)},
                            device_id_type=MESH)
    ends = (me == 0).astype(jnp.int32) + (me == n_fs - 1).astype(jnp.int32)
    pl.semaphore_wait(barrier, n_grp - 1 + n_tp - 1 + 2 - ends)

    def send_own(q):
        for copy in local_copies(q, 0):
            copy.wait()

        @pl.when(me < n_fs - 1)
        def _():
            z_own(q, True).start()

        @pl.when(me > 0)
        def _():
            z_own(q, False).start()

    def relay(q, d):
        for side in (True, False):
            src = me - d if side else me + d

            @pl.when((src >= 0) & (src < n_fs))
            def _(src=src, side=side):
                z_copy(q, src, side).wait_recv()

                @pl.when(me < n_fs - 1 if side else me > 0)
                def _():
                    z_copy(q, src, side).start()

                for j in range(1, n_grp):
                    y_copy(q, src, j).start()

    def norm_tokens():
        tok_copy.wait()
        step = 64

        @pl.loop(0, tok.shape[0] // step)
        def _(r):
            at = pl.ds(pl.multiple_of(r * step, step), step)
            values = tok[at, :].astype(jnp.float32)
            scale = lax.rsqrt(jnp.mean(values * values, axis=1, keepdims=True) + EPS)
            normed[at, :] = (values * scale * gain_ref[...]).astype(jnp.bfloat16)

    def compute(q):
        for j in range(1, n_grp):
            for copy in local_copies(q, j):
                copy.wait()
            for src in range(n_fs):
                @pl.when(src != me)
                def _():
                    y_arrival(q, src, j).wait_recv()
        for g in range(n_grp):
            if q < p_up:
                up = jnp.dot(normed[...], ubuf[q, g], preferred_element_type=jnp.float32)
                at = (q * n_grp + g) * c_up
                hidden[:, at:at + c_up] = jnp.square(jnp.maximum(up, 0.0)).astype(jnp.bfloat16)
            else:
                part = jnp.dot(hidden[...], dbuf[q - p_up, g], preferred_element_type=jnp.float32)
                part = part.astype(jnp.bfloat16)
                for i in range(per_grp):
                    sbuf[q - p_up, g * per_grp + i] = part[:, i * LANES:(i + 1) * LANES]
        if q >= p_up:
            for j in range(1, n_tp):
                part_copy(q - p_up, j).start()

    def finish(q):
        total = sbuf[q, tp].astype(jnp.float32)
        for j in range(1, n_tp):
            part_copy(q, j).wait_recv()
            total = total + rbuf[q, j - 1].astype(jnp.float32)
        out_ref[:, q * LANES:(q + 1) * LANES] = total

    lag = n_fs + 1
    for k in range(pieces + lag):
        if k < pieces:
            send_own(k)
        for q in range(pieces):
            if 1 <= k - q <= n_fs - 1:
                relay(q, k - q)
        if k == 1:
            norm_tokens()
        if 0 <= k - lag < pieces:
            compute(k - lag)
        if k - lag - 1 >= p_up:
            finish(k - lag - 1 - p_up)
    finish(p_dn - 1)

    for q in range(pieces):
        @pl.when(me < n_fs - 1)
        def _():
            z_own(q, True).wait_send()

        @pl.when(me > 0)
        def _():
            z_own(q, False).wait_send()

        for d in range(1, n_fs):
            for side in (True, False):
                src = me - d if side else me + d

                @pl.when((src >= 0) & (src < n_fs))
                def _(src=src, side=side):
                    @pl.when(me < n_fs - 1 if side else me > 0)
                    def _():
                        z_copy(q, src, side).wait_send()

                    for j in range(1, n_grp):
                        y_copy(q, src, j).wait_send()
    for q in range(p_dn):
        for j in range(1, n_tp):
            part_copy(q, j).wait_send()


def shards(n_grp, n_fs, n_tp, tokens, pre_gain, up_weight, down_weight, post_gain):
    rows, width = tokens.shape
    own_width = post_gain.shape[0]
    ff = up_weight.shape[1]
    c_up = min(2 * LANES, ff // n_grp)
    p_up = ff // (n_grp * c_up)
    p_dn = own_width // LANES
    c_dn = n_tp // n_grp * LANES
    pieces = p_up + p_dn
    sizes = (n_grp, n_fs, n_tp, p_up, p_dn, c_up)
    vmem = pltpu.VMEM
    dma = pltpu.SemaphoreType.DMA
    total = pl.pallas_call(
        functools.partial(layer_kernel, sizes),
        out_shape=jax.ShapeDtypeStruct((rows, own_width), jnp.float32),
        in_specs=[
            pl.BlockSpec(memory_space=pl.ANY),
            pl.BlockSpec(memory_space=pltpu.VMEM),
            pl.BlockSpec(memory_space=pl.ANY),
            pl.BlockSpec(memory_space=pl.ANY),
        ],
        out_specs=pl.BlockSpec(memory_space=pltpu.VMEM),
        scratch_shapes=[
            vmem((rows, width), jnp.bfloat16),
            vmem((rows, width), jnp.bfloat16),
            vmem((p_up, n_grp, width, c_up), jnp.bfloat16),
            vmem((p_dn, n_grp, ff, c_dn), jnp.bfloat16),
            vmem((rows, ff), jnp.bfloat16),
            vmem((p_dn, n_tp, rows, LANES), jnp.bfloat16),
            vmem((p_dn, n_tp - 1, rows, LANES), jnp.bfloat16),
            dma,
            dma((p_up, n_grp)),
            dma((p_dn, n_grp, n_tp // n_grp)),
            dma((pieces, n_fs)),
            dma((pieces, n_grp, n_fs)),
            dma((pieces, n_fs + 1)),
            dma((pieces, n_grp, n_fs)),
            dma((p_dn, n_tp - 1)),
            dma((p_dn, n_tp - 1)),
        ],
        compiler_params=pltpu.CompilerParams(
            collective_id=0, has_side_effects=True, vmem_limit_bytes=60 * 1024 * 1024),
        cost_estimate=pl.CostEstimate(
            flops=4 * rows * width * ff, bytes_accessed=16 * rows * width, transcendentals=rows),
    )(tokens, pre_gain.reshape(1, -1), up_weight, down_weight)
    squares = lax.psum(jnp.sum(total * total, axis=1), "tp")
    factor = lax.rsqrt(squares / (n_tp * own_width) + EPS)
    return (total * factor[:, None] * post_gain).astype(jnp.bfloat16)


def solution(mesh):
    in_specs = (P(("grp", "fs"), None), P(), P("fs", "tp"), P(("tp", "fs"), None), P("tp"))
    out_specs = P(("grp", "fs"), "tp")
    body = functools.partial(shards, mesh.shape["grp"], mesh.shape["fs"], mesh.shape["tp"])
    return jax.shard_map(body, mesh=mesh, in_specs=in_specs, out_specs=out_specs, check_vma=False)
```

time: 383 us -> 185 us (0.48)
  waiting for transfers between devices: 339 us -> 0 us
  Pallas kernels: 0 us -> 174 us
  matrix products: 20.6 us -> 0 us
  between operations: 13.1 us -> 0.03 us
    all_gather x2 -> x0, waiting for transfers between devices: 302 us -> none  [the longest x1 152 us: shards(): full_up = lax.all_gather(up_weight, 'fs', axis=0, tiled=True)]
    pallas_call x0 -> x1, Pallas kernels: none -> 174 us  [shards(): pl.pallas_call(functools.partial(layer_kernel, sizes), out_shape=jax.Shap...]
    reduce_scatter x1 -> x0, waiting for transfers between devices: 36.1 us -> none  [shards(): lax.psum_scatter(partial_terms.astype(jnp.bfloat16), 'tp', scatter_dimens...]
    dot_general x1 -> x0, matrix products: 20.6 us -> none  [shards(): jnp.dot(hidden, full_down, preferred_element_type=jnp.float32)]
  transfers between devices with their start and end apart: 3 -> 0, of which waited for: 3 -> 0; matrix products, arithmetic and copies ran while one was open for 0% -> 0% of each run, Pallas kernels for 0% -> 0%
where the time goes in v1:
time: 185 us
  Pallas kernels  174 us (94%)
  blocking collectives  7.77 us (4%)
  other arithmetic  2.8 us (2%)
    pallas_call x1, Pallas kernels, shards(): pl.pallas_call(functools.partial(layer_kernel, sizes), out_shape=jax.Shap...  174 us
    psum x1, blocking collectives, shards(): squares = lax.psum(jnp.sum(total * total, axis=1), 'tp')  7.77 us

profile of v1, /device:TPU:0, one launch (start us, length us, event | category | flops | bytes accessed | tf_op | source)
XLA Modules:
  0.0 184.9 jit_solution(13463020123595365730)
XLA Ops:
  0.0 174.3 %shard_map.55 = f32[768,512]{1,0:T(8,128)} custom-call(bf16[768,2048]{1,0:T(8,128)(2,1)} %tok_hbm.1, f32[1,2048]{1,0:T(1,128)} %bitcast.1, bf16[512,2048]{1,0:T(8,128)(2,1)} %up_hbm.1, bf16[512,2048]{1,0:T(8,128)(2,1)} %down_hbm.1), custom_call_target="tpu_custom_call" | custom-call | flops 12884901888 | bytes 25165824 | tf_op jit(solution)/shard_map/pallas_call | solution.py:230
  174.3 0.0 copy-start
  174.3 0.0 copy-start.1
  174.3 1.7 multiply_reduce_fusion
  176.0 7.8 %psum.7 = f32[768]{0:T(1024)S(1)} all-reduce(f32[768]{0:T(1024)S(1)} %multiply_reduce_fusion), channel_id=1, replica_groups=mesh['grp'=2,'fs'=4,'tp'=4] {'tp'}, use_global_device_ids=true, to_apply=%region_1.0 | all-reduce | flops 768 | bytes 6144 | tf_op jit(solution)/shard_map/psum | solution.py:263
  183.8 0.0 copy-done
  183.8 0.0 copy-done.1
  183.8 1.1 multiply_convert_fusion
  (1 shorter events, 0.0 us)
Async XLA Ops:
  174.3 9.5 %copy-start = (f32[768,512]{1,0:T(8,128)S(1)}, f32[768,512]{1,0:T(8,128)}, u32[]{:S(2)}) copy-start(f32[768,512]{1,0:T(8,128)} %shard_map.55) | copy-start | bytes 4718596
  174.3 9.5 %copy-start.1 = (f32[512]{0:T(512)S(1)}, f32[512]{0:T(512)}, u32[]{:S(2)}) copy-start(f32[512]{0:T(512)} %param.9) | copy-start | bytes 6148

commit v2 on v1

--- a/solution.py
+++ b/solution.py
@@ -12,10 +12,11 @@
 LANES = 128
 
 
-def layer_kernel(sizes, tok_hbm, gain_ref, up_hbm, down_hbm, out_ref,
-                 tok, normed, ubuf, dbuf, hidden, sbuf, rbuf,
-                 tok_sem, lup_sem, ldn_sem, zrecv, yrecv, zsend, ysend, rsend, rrecv):
-    n_grp, n_fs, n_tp, p_up, p_dn, c_up = sizes
+def layer_kernel(sizes, tok_hbm, gain_ref, up_hbm, down_hbm, post_ref, out_ref,
+                 tok, normed, ubuf, dbuf, hidden, sbuf, rbuf, total_buf, square_buf, own_sq, peer_sq,
+                 tok_sem, lup_sem, ldn_sem, zrecv, yrecv, zsend, ysend, rsend, rrecv,
+                 sq_send, sq_recv):
+    n_grp, n_fs, n_tp, p_up, p_dn, c_up, splits = sizes
     per_grp = n_tp // n_grp
     pieces = p_up + p_dn
     grp = lax.axis_index("grp")
@@ -73,12 +74,23 @@
             send_sem=ysend.at[q, j, src], recv_sem=yrecv.at[q, j, src],
             device_id={"grp": g}, device_id_type=MESH)
 
-    def part_copy(q, j):
+    def row_blocks(q):
+        count = splits if q == p_dn - 1 else 1
+        height = tok.shape[0] // count
+        return [(b, pl.ds(b * height, height)) for b in range(count)]
+
+    def part_copy(q, j, b, at):
         to = lax.rem(tp + j, n_tp)
         return pltpu.make_async_remote_copy(
-            src_ref=sbuf.at[q, to], dst_ref=rbuf.at[q, j - 1],
-            send_sem=rsend.at[q, j - 1], recv_sem=rrecv.at[q, j - 1],
+            src_ref=sbuf.at[q, to, at, :], dst_ref=rbuf.at[q, j - 1, at, :],
+            send_sem=rsend.at[q, j - 1, b], recv_sem=rrecv.at[q, j - 1, b],
             device_id={"tp": to}, device_id_type=MESH)
+
+    def square_copy(j):
+        return pltpu.make_async_remote_copy(
+            src_ref=own_sq, dst_ref=peer_sq.at[j - 1],
+            send_sem=sq_send.at[j - 1], recv_sem=sq_recv.at[j - 1],
+            device_id={"tp": lax.rem(tp + j, n_tp)}, device_id_type=MESH)
 
     tok_copy = pltpu.make_async_copy(tok_hbm, tok, tok_sem)
     for q in range(pieces):
@@ -153,28 +165,36 @@
                 @pl.when(src != me)
                 def _():
                     y_arrival(q, src, j).wait_recv()
-        for g in range(n_grp):
-            if q < p_up:
+        if q < p_up:
+            for g in range(n_grp):
                 up = jnp.dot(normed[...], ubuf[q, g], preferred_element_type=jnp.float32)
                 at = (q * n_grp + g) * c_up
                 hidden[:, at:at + c_up] = jnp.square(jnp.maximum(up, 0.0)).astype(jnp.bfloat16)
-            else:
-                part = jnp.dot(hidden[...], dbuf[q - p_up, g], preferred_element_type=jnp.float32)
+            return
+        blocks = row_blocks(q - p_up)
+        for b, at in blocks:
+            for g in range(n_grp):
+                part = jnp.dot(hidden[at, :], dbuf[q - p_up, g], preferred_element_type=jnp.float32)
                 part = part.astype(jnp.bfloat16)
                 for i in range(per_grp):
-                    sbuf[q - p_up, g * per_grp + i] = part[:, i * LANES:(i + 1) * LANES]
-        if q >= p_up:
+                    sbuf[q - p_up, g * per_grp + i, at, :] = part[:, i * LANES:(i + 1) * LANES]
+            if b > 0:
+                for j in range(1, n_tp):
+                    part_copy(q - p_up, j, *blocks[b - 1]).start()
+        for j in range(1, n_tp):
+            part_copy(q - p_up, j, *blocks[-1]).start()
+
+    def finish(q):
+        for b, at in row_blocks(q):
+            total = sbuf[q, tp, at, :].astype(jnp.float32)
             for j in range(1, n_tp):
-                part_copy(q - p_up, j).start()
-
-    def finish(q):
-        total = sbuf[q, tp].astype(jnp.float32)
-        for j in range(1, n_tp):
-            part_copy(q, j).wait_recv()
-            total = total + rbuf[q, j - 1].astype(jnp.float32)
-        out_ref[:, q * LANES:(q + 1) * LANES] = total
-
-    lag = n_fs + 1
+                part_copy(q, j, b, at).wait_recv()
+                total = total + rbuf[q, j - 1, at, :].astype(jnp.float32)
+            total_buf[at, q * LANES:(q + 1) * LANES] = total
+            square = total * total
+            square_buf[at, :] = square if q == 0 else square_buf[at, :] + square
+
+    lag = n_fs
     for k in range(pieces + lag):
         if k < pieces:
             send_own(k)
@@ -189,6 +209,21 @@
             finish(k - lag - 1 - p_up)
     finish(p_dn - 1)
 
+    rows = tok.shape[0]
+    own = jnp.sum(square_buf[...].T, axis=0, keepdims=True)
+    own_sq[...] = jnp.broadcast_to(own, own_sq.shape)
+    for j in range(1, n_tp):
+        square_copy(j).start()
+    squares = own_sq[...]
+    for j in range(1, n_tp):
+        square_copy(j).wait_recv()
+        squares = squares + peer_sq[j - 1]
+    factor = lax.rsqrt(squares / (n_tp * own_width) + EPS)
+    factor = jnp.broadcast_to(factor[0:1, :], (LANES, rows)).T
+    for q in range(p_dn):
+        at = slice(q * LANES, (q + 1) * LANES)
+        out_ref[:, at] = (total_buf[:, at] * factor * post_ref[:, at]).astype(out_ref.dtype)
+
     for q in range(pieces):
         @pl.when(me < n_fs - 1)
         def _():
@@ -212,7 +247,10 @@
                         y_copy(q, src, j).wait_send()
     for q in range(p_dn):
         for j in range(1, n_tp):
-            part_copy(q, j).wait_send()
+            for b, at in row_blocks(q):
+                part_copy(q, j, b, at).wait_send()
+    for j in range(1, n_tp):
+        square_copy(j).wait_send()
 
 
 def shards(n_grp, n_fs, n_tp, tokens, pre_gain, up_weight, down_weight, post_gain):
@@ -224,17 +262,19 @@
     p_dn = own_width // LANES
     c_dn = n_tp // n_grp * LANES
     pieces = p_up + p_dn
-    sizes = (n_grp, n_fs, n_tp, p_up, p_dn, c_up)
+    splits = 1
+    sizes = (n_grp, n_fs, n_tp, p_up, p_dn, c_up, splits)
     vmem = pltpu.VMEM
     dma = pltpu.SemaphoreType.DMA
-    total = pl.pallas_call(
+    return pl.pallas_call(
         functools.partial(layer_kernel, sizes),
-        out_shape=jax.ShapeDtypeStruct((rows, own_width), jnp.float32),
+        out_shape=jax.ShapeDtypeStruct((rows, own_width), jnp.bfloat16),
         in_specs=[
             pl.BlockSpec(memory_space=pl.ANY),
             pl.BlockSpec(memory_space=pltpu.VMEM),
             pl.BlockSpec(memory_space=pl.ANY),
             pl.BlockSpec(memory_space=pl.ANY),
+            pl.BlockSpec(memory_space=pltpu.VMEM),
         ],
         out_specs=pl.BlockSpec(memory_space=pltpu.VMEM),
         scratch_shapes=[
@@ -245,6 +285,10 @@
             vmem((rows, ff), jnp.bfloat16),
             vmem((p_dn, n_tp, rows, LANES), jnp.bfloat16),
             vmem((p_dn, n_tp - 1, rows, LANES), jnp.bfloat16),
+            vmem((rows, own_width), jnp.float32),
+            vmem((rows, LANES), jnp.float32),
+            vmem((8, rows), jnp.float32),
+            vmem((n_tp - 1, 8, rows), jnp.float32),
             dma,
             dma((p_up, n_grp)),
             dma((p_dn, n_grp, n_tp // n_grp)),
@@ -252,17 +296,16 @@
             dma((pieces, n_grp, n_fs)),
             dma((pieces, n_fs + 1)),
             dma((pieces, n_grp, n_fs)),
-            dma((p_dn, n_tp - 1)),
-            dma((p_dn, n_tp - 1)),
+            dma((p_dn, n_tp - 1, splits)),
+            dma((p_dn, n_tp - 1, splits)),
+            dma((n_tp - 1,)),
+            dma((n_tp - 1,)),
         ],
         compiler_params=pltpu.CompilerParams(
             collective_id=0, has_side_effects=True, vmem_limit_bytes=60 * 1024 * 1024),
         cost_estimate=pl.CostEstimate(
             flops=4 * rows * width * ff, bytes_accessed=16 * rows * width, transcendentals=rows),
-    )(tokens, pre_gain.reshape(1, -1), up_weight, down_weight)
-    squares = lax.psum(jnp.sum(total * total, axis=1), "tp")
-    factor = lax.rsqrt(squares / (n_tp * own_width) + EPS)
-    return (total * factor[:, None] * post_gain).astype(jnp.bfloat16)
+    )(tokens, pre_gain.reshape(1, -1), up_weight, down_weight, post_gain.reshape(1, -1))
 
 
 def solution(mesh):

time: 185 us -> 173 us (0.935)
  blocking collectives: 7.77 us -> 0 us
  Pallas kernels: 174 us -> 170 us
  other arithmetic: 2.8 us -> 0 us
  local copies, waits for them, and re-layouts: 0.01 us -> 2.06 us
    psum x1 -> x0, blocking collectives: 7.77 us -> none  [shards(): squares = lax.psum(jnp.sum(total * total, axis=1), 'tp')]
    pallas_call x1, Pallas kernels: 174 us -> 170 us  [shards(): pl.pallas_call(functools.partial(layer_kernel, sizes), out_shape=jax.Shap...]
    unnamed x4 -> x1, local copies, waits for them, and re-layouts: 0.01 us -> 2.06 us
where the time goes in v2:
time: 173 us; the launch traced here: 172 us
  Pallas kernels  170 us (98%)
  local copies, waits for them, and re-layouts  2.06 us (1%)
    pallas_call x1, Pallas kernels, shards(): pl.pallas_call(functools.partial(layer_kernel, sizes), out_shape=jax.Shap...  170 us

profile of v2, /device:TPU:0, one launch (start us, length us, event | category | flops | bytes accessed | tf_op | source)
XLA Modules:
  0.0 172.5 jit_solution(7099086181452258279)
XLA Ops:
  0.0 170.4 %shard_map.55 = bf16[768,512]{1,0:T(8,128)(2,1)} custom-call(bf16[768,2048]{1,0:T(8,128)(2,1)} %tok_hbm.1, f32[1,2048]{1,0:T(1,128)} %bitcast.2, bf16[512,2048]{1,0:T(8,128)(2,1)} %up_hbm.1, bf16[512,2048]{1,0:T(8,128)(2,1)} %down_hbm.1, f32[1,512]{1,0:T(1,128)} %bitcast.3), custom_call_target="tpu_custom_call" | custom-call | flops 12884901888 | bytes 25165824 | tf_op jit(solution)/shard_map/pallas_call | solution.py:269
  170.4 2.1 %copy.7 = bf16[768,512]{1,0:T(8,128)(2,1)} copy(bf16[768,512]{1,0:T(8,128)(2,1)} %shard_map.55) | data formatting | bytes 1572864
